TPU v7x, 32 devices: a whole 2x2x4 slice. The times are simulated.
32 devices in a mesh: ep: 8 (over z, x), tp: 4 (over y, core).
Axes of the slice: x: 2, y: 2, z: 4, core: 2. Of those that a mesh axis runs over, the one named last changes fastest.
Arguments:
- tokens: bfloat16 [64, 4096], P('ep', 'tp'), may hold values from -6 to 6
- norm_gain: float32 [4096], replicated, may hold values from 0.1 to 1.9
- route_experts: int32 [64, 2], P('ep'), may hold values from 0 to 15, all different within a row; in each aligned block of 8 rows (0 to 7, 8 to 15, ...) at most 2 rows name the same one
- route_logits: float32 [64, 2], P('ep'), may hold values from -4 to 4
- expert_gate: bfloat16 [16, 4096, 1024], P('ep', None, 'tp'), may hold values from -0.09375 to 0.09375
- expert_up: bfloat16 [16, 4096, 1024], P('ep', None, 'tp'), may hold values from -0.09375 to 0.09375
- expert_down: bfloat16 [16, 1024, 4096], P('ep', 'tp'), may hold values from -0.1875 to 0.1875
- dense_gate: bfloat16 [4096, 1024], P(None, 'tp'), may hold values from -0.09375 to 0.09375
- dense_up: bfloat16 [4096, 1024], P(None, 'tp'), may hold values from -0.09375 to 0.09375
- dense_down: bfloat16 [1024, 4096], P('tp'), may hold values from -0.1875 to 0.1875
- mix_weight: float32 [4096], replicated, may hold values from -0.09375 to 0.09375
- out_gain: float32 [4096], P('tp'), may hold values from 0.1 to 1.9
Outputs:
- result: bfloat16 [64, 4096], P('ep', 'tp')
Inputs may be any that keep to these rules, and one draw needn't show every extreme that they name: `route_experts`: each row names 2 different experts; the 8 rows of one index of ep (aligned blocks) name any one expert at most 2 times, and some block names some expert exactly 2 times; every expert is named somewhere.
All inputs are finite; a program needn't handle non-finite values.
Results may differ from a plain program's by a relative error of at most 0.0025.
Values may be sent and summed in bfloat16 or wider, within the bound.
A program may use at most 64 MiB of HBM per device.

v0:
```python
import jax
import jax.numpy as jnp
from jax import lax
from jax.sharding import PartitionSpec as P

CAP = 2


norm_eps = 1e-06


def shards(
    tokens,
    norm_gain,
    route_experts,
    route_logits,
    expert_gate,
    expert_up,
    expert_down,
    dense_gate,
    dense_up,
    dense_down,
    mix_weight,
    out_gain,
):
    tok_rows, width_part = tokens.shape
    groups = lax.axis_size("tp")
    width = width_part * groups
    whole_rows = lax.all_gather(tokens, "tp", axis=1, tiled=True).astype(jnp.float32)
    normed = (
        whole_rows
        * lax.rsqrt(jnp.mean(whole_rows * whole_rows, axis=1, keepdims=True) + norm_eps)
        * norm_gain
    ).astype(jnp.bfloat16)
    weights = jax.nn.softmax(route_logits, axis=-1)
    top_count = route_experts.shape[1]
    local_experts = expert_gate.shape[0]
    peer_count = lax.axis_size("ep")
    experts = local_experts * peer_count
    dense_hidden = (
        jax.nn.silu(jnp.dot(normed, dense_gate, preferred_element_type=jnp.float32))
        * jnp.dot(normed, dense_up, preferred_element_type=jnp.float32)
    ).astype(jnp.bfloat16)
    dense_out = lax.psum_scatter(
        jnp.dot(dense_hidden, dense_down, preferred_element_type=jnp.float32),
        "tp",
        scatter_dimension=1,
        tiled=True,
    )
    mix_gate = jax.nn.sigmoid(
        jnp.dot(normed.astype(jnp.float32), mix_weight, precision=lax.Precision.HIGHEST)
    )
    flat_routes = route_experts.reshape(-1)
    expert_ids = jnp.arange(experts, dtype=jnp.int32)
    capacity = CAP
    slot_count = experts * capacity
    route_hits = (flat_routes[:, None] == expert_ids[None, :]).astype(jnp.int32)
    before = jnp.cumsum(route_hits, axis=0) - route_hits
    slot_rank = jnp.sum(before * route_hits, axis=1)
    position = flat_routes * capacity + slot_rank
    onehot_place = (position[:, None] == jnp.arange(slot_count, dtype=jnp.int32)[None, :]).astype(
        jnp.float32
    )
    placing = jnp.sum(onehot_place.reshape(tok_rows, top_count, slot_count), axis=1).T.astype(
        jnp.bfloat16
    )
    outgoing = jnp.dot(placing, normed, preferred_element_type=jnp.float32).astype(jnp.bfloat16)
    received = lax.all_to_all(outgoing, "ep", split_axis=0, concat_axis=0, tiled=True)
    arranged = (
        received.reshape(peer_count, local_experts, capacity, width)
        .transpose(1, 0, 2, 3)
        .reshape(local_experts, peer_count * capacity, width)
    )
    gate_act = jnp.einsum("erd,edf->erf", arranged, expert_gate, preferred_element_type=jnp.float32)
    up_act = jnp.einsum("erd,edf->erf", arranged, expert_up, preferred_element_type=jnp.float32)
    hidden = (jax.nn.silu(gate_act) * up_act).astype(jnp.bfloat16)
    partial_value = jnp.einsum(
        "erf,efd->erd", hidden, expert_down, preferred_element_type=jnp.float32
    )
    summed = lax.psum_scatter(partial_value, "tp", scatter_dimension=2, tiled=True)
    back_send = (
        summed.reshape(local_experts, peer_count, capacity, width_part)
        .transpose(1, 0, 2, 3)
        .reshape(slot_count, width_part)
    )
    returned = lax.all_to_all(back_send, "ep", split_axis=0, concat_axis=0, tiled=True)
    combine_map = jnp.sum(
        (onehot_place * weights.reshape(-1)[:, None]).reshape(tok_rows, top_count, slot_count),
        axis=1,
    )
    expert_mix = jnp.dot(combine_map, returned, precision=lax.Precision.HIGHEST)
    combined = expert_mix + mix_gate[:, None] * dense_out
    squares_out = lax.psum(jnp.sum(combined * combined, axis=1), "tp")
    result = combined * lax.rsqrt(squares_out[:, None] / width + norm_eps) * out_gain
    return result.astype(jnp.bfloat16)


def solution(mesh):
    placed = (
        P("ep", "tp"),
        P(),
        P("ep", None),
        P("ep", None),
        P("ep", None, "tp"),
        P("ep", None, "tp"),
        P("ep", "tp", None),
        P(None, "tp"),
        P(None, "tp"),
        P("tp", None),
        P(),
        P("tp"),
    )
    return jax.shard_map(
        shards, mesh=mesh, in_specs=placed, out_specs=P("ep", "tp"), check_vma=False
    )
```

profile of v0, /device:TPU:0, one launch (start us, length us, event | category | flops | bytes accessed | tf_op | source)
XLA Modules:
  0.0 100.3 jit_solution(16466553001258629282)
XLA Ops:
  6.5 0.0 copy-start
  6.5 0.0 reduce-scatter.3.cloned.1.call-start
  6.5 0.8 reduce_max.9
  7.4 0.7 fusion.26
  8.1 0.7 fusion.25
  8.8 0.8 copy.34
  9.5 0.1 eq.30
  9.6 0.1 fusion.22
  9.7 0.2 select_reduce_fusion.1
  9.9 0.1 reduce_sum.57
  10.0 0.1 copy.36
  10.1 6.5 %all_gather.3 = bf16[8,4096]{1,0:T(8,128)(2,1)S(1)} all-gather(bf16[8,1024]{1,0:T(8,128)(2,1)} %param.12), channel_id=1, replica_groups=mesh['ep'=8,'tp'=4] {'tp'}, dimensions={1}, use_global_device_ids=true | all-gather | bytes 81920 | tf_op jit(solution)/shard_map/all_gather | solution.py:29
  16.5 0.1 fusion.8
  16.7 0.1 convert_reduce_fusion
  16.8 1.0 convolution_convert_fusion
  17.8 0.1 all_to_all.14
  17.9 15.5 %all_to_all.21 = bf16[8,4,4096]{2,1,0:T(4,128)(2,1)S(1)} all-to-all(bf16[8,4,4096]{2,1,0:T(4,128)(2,1)S(1)} %all_to_all.14), channel_id=1, replica_groups=mesh['ep'=8,'tp'=4] {'ep'}, dimensions={0} | all-to-all | bytes 524288 | tf_op jit(solution)/shard_map/all_to_all | solution.py:68
  33.4 0.1 reshape.67
  33.6 0.2 copy.41
  33.8 0.1 reshape.68
  33.9 2.8 %fusion.35 = f32[2,16,256]{2,1,0:T(8,128)S(1)} fusion(bf16[2,16,4096]{2,1,0:T(8,128)(2,1)S(1)} %reshape.68, bf16[2,4096,256]{2,1,0:T(8,128)(2,1)} %param.16), kind=kOutput, calls=%fused_computation.49 | convolution fusion | flops 67108864 | bytes 4489216 | tf_op jit(solution)/shard_map/erd,edf->erf/dot_general | solution.py:74
  36.7 0.0 copy-start.1
  36.7 5.6 %fusion.1 = f32[2,16,4096]{2,1,0:T(8,128)} fusion(bf16[2,256,4096]{2,1,0:T(8,128)(2,1)} %param.18, bf16[2,16,4096]{2,1,0:T(8,128)(2,1)S(1)} %reshape.68, bf16[2,4096,256]{2,1,0:T(8,128)(2,1)} %param.17, f32[2,16,256]{2,1,0:T(8,128)S(1)} %fusion.35), kind=kOutput, calls=%fused_computation.4 | convolution fusion | flops 134266880 | bytes 9207808 | tf_op jit(solution)/shard_map/erf,efd->erd/dot_general | solution.py:77
  42.3 0.0 copy-start.3
  42.3 0.0 reduce-scatter.3.cloned.1.call-update
  42.3 0.0 copy-start.2
  42.3 0.0 reduce-scatter.5.cloned.1.call-start
  42.4 0.0 copy-done.1
  42.4 2.0 %fusion.31 = f32[8,256]{1,0:T(8,128)S(1)} fusion(bf16[4096,256]{1,0:T(8,128)(2,1)} %param.19, bf16[8,4096]{1,0:T(8,128)(2,1)S(1)} %all_gather.3, f32[4096]{0:T(1024)S(1)} %copy-done.1, f32[8]{0:T(128)S(1)} %add_rsqrt_fusion.1), kind=kOutput, calls=%fused_computation.48 | convolution fusion | flops 16908288 | bytes 2187296 | tf_op jit(solution)/shard_map/dot_general | solution.py:41
  44.4 0.0 copy-done
  44.4 3.6 %fusion.3 = f32[8,4096]{1,0:T(8,128)} fusion(bf16[256,4096]{1,0:T(8,128)(2,1)S(1)} %copy-done, bf16[4096,256]{1,0:T(8,128)(2,1)} %param.20, f32[8,256]{1,0:T(8,128)S(1)} %fusion.31, bf16[8,4096]{1,0:T(8,128)(2,1)S(1)} %all_gather.3, f32[4096]{0:T(1024)S(1)} %copy-done.1, f32[8]{0:T(128)S(1)} %add_rsqrt_fusion.1), kind=kOutput, calls=%fused_computation.7 | convolution fusion | flops 33697792 | bytes 4415520 | tf_op jit(solution)/shard_map/dot_general | solution.py:45
  47.9 0.0 reduce-scatter.5.cloned.1.call-update
  48.0 15.9 %reduce-scatter.3.cloned.1.call-done = f32[2,16,1024]{2,1,0:T(8,128)} async-done(((f32[2,16,4096]{2,1,0:T(8,128)}), f32[2,16,1024]{2,1,0:T(8,128)}) %reduce-scatter.3.cloned.1.call-update) | async-done | bytes 131088 | tf_op jit(solution)/shard_map/reduce_scatter | solution.py:80
  63.9 1.0 reshape.69
  64.9 0.7 copy.39
  65.6 5.5 %all-to-all-start.1 = ((f32[8,4,1024]{2,1,0:T(4,128)}), f32[8,4,1024]{2,1,0:T(4,128)S(1)}, u32[]{:S(2)}, u32[]{:S(2)}) async-start(f32[8,4,1024]{2,1,0:T(4,128)} %copy.39), calls=%async_computation.2 | async-start | bytes 262144 | tf_op jit(solution)/shard_map/all_to_all | solution.py:86
  71.1 0.0 copy-done.3
  71.1 0.3 fusion.7
  71.4 7.1 %all-to-all-done.1 = f32[8,4,1024]{2,1,0:T(4,128)S(1)} async-done(((f32[8,4,1024]{2,1,0:T(4,128)}), f32[8,4,1024]{2,1,0:T(4,128)S(1)}, u32[]{:S(2)}, u32[]{:S(2)}) %all-to-all-start.1) | async-done | bytes 131104 | tf_op jit(solution)/shard_map/all_to_all | solution.py:86
  78.5 7.5 %reduce-scatter.5.cloned.1.call-done = f32[8,1024]{1,0:T(8,128)} async-done(((f32[8,4096]{1,0:T(8,128)}), f32[8,1024]{1,0:T(8,128)}) %reduce-scatter.5.cloned.1.call-update) | async-done | bytes 32784 | tf_op jit(solution)/shard_map/reduce_scatter | solution.py:44
  86.0 1.1 %multiply_reduce_fusion = (f32[8]{0:T(128)S(1)}, f32[8,1024]{1,0:T(8,128)S(1)}) fusion(f32[8,1024]{1,0:T(8,128)} %reduce-scatter.5.cloned.1.call-done, f32[8]{0:T(128)S(1)} %fusion.7, f32[8,32]{1,0:T(8,128)S(1)} %get-tuple-element.6, f32[32,1024]{1,0:T(8,128)S(1)} %all_to_all.18), kind=kOutput, calls=%fused_computation.20 | convolution fusion | flops 3178488 | bytes 197696 | tf_op jit(solution)/shard_map/dot_general | solution.py:91
  87.0 5.8 %psum.7 = f32[8]{0:T(128)S(1)} all-reduce(f32[8]{0:T(128)S(1)} %get-tuple-element.7), channel_id=1, replica_groups=mesh['ep'=8,'tp'=4] {'tp'}, use_global_device_ids=true, to_apply=%region_10.11 | all-reduce | flops 8 | bytes 64 | tf_op jit(solution)/shard_map/psum | solution.py:93
  92.8 0.0 copy-done.2
  92.8 0.7 multiply_convert_fusion
  (6 shorter events, 0.1 us)
Async XLA Ops:
  6.5 37.8 %copy-start = (bf16[256,4096]{1,0:T(8,128)(2,1)S(1)}, bf16[256,4096]{1,0:T(8,128)(2,1)}, u32[]{:S(2)}) copy-start(bf16[256,4096]{1,0:T(8,128)(2,1)} %param.21) | copy-start | bytes 6291460
  6.5 57.3 %reduce-scatter.3.cloned.1.call-start = ((), (), s32[]{:S(2)}) async-start(), calls=%async_computation.4 | async-start | bytes 655360 | tf_op jit(solution)/shard_map/reduce_scatter | solution.py:80
  36.7 5.6 %copy-start.1 = (f32[4096]{0:T(1024)S(1)}, f32[4096]{0:T(1024)}, u32[]{:S(2)}) copy-start(f32[4096]{0:T(1024)} %param.13) | copy-start | bytes 49156
  42.3 28.8 %copy-start.3 = (f32[4096]{0:T(1024)S(1)}, f32[4096]{0:T(1024)}, u32[]{:S(2)}) copy-start(f32[4096]{0:T(1024)} %param.22) | copy-start | bytes 49156
  42.3 50.5 %copy-start.2 = (f32[1024]{0:T(1024)S(1)}, f32[1024]{0:T(1024)}, u32[]{:S(2)}) copy-start(f32[1024]{0:T(1024)} %param.23) | copy-start | bytes 12292
  42.3 43.6 %reduce-scatter.5.cloned.1.call-start = ((), (), s32[]{:S(2)}) async-start(), calls=%async_computation.5 | async-start | bytes 163840 | tf_op jit(solution)/shard_map/reduce_scatter | solution.py:44
  65.6 12.8 %all-to-all-start.1 = ((f32[8,4,1024]{2,1,0:T(4,128)}), f32[8,4,1024]{2,1,0:T(4,128)S(1)}, u32[]{:S(2)}, u32[]{:S(2)}) async-start(f32[8,4,1024]{2,1,0:T(4,128)} %copy.39), calls=%async_computation.2 | async-start | bytes 262144 | tf_op jit(solution)/shard_map/all_to_all | solution.py:86
Sparse Core Ops, SparseCore 0:
  42.4 21.3 reduce-scatter.2
  66.3 19.6 reduce-scatter.4
where the time goes:
time: 101 us; the launch traced here: 100 us
  waiting for transfers between devices  30.4 us (30%)
  blocking collectives  27.7 us (27%)
  matrix products  16.3 us (16%)
  between operations  13.5 us (13%)
  starting transfers between devices  5.54 us (5%)
  other arithmetic  3.46 us (3%)
  local copies, waits for them, and re-layouts  3.35 us (3%)
    reduce_scatter x1, waiting for transfers between devices, shards(): lax.psum_scatter(partial_value, 'tp', scatter_dimension=2, tiled=True)  15.9 us
    all_to_all x1, blocking collectives, shards(): lax.all_to_all(outgoing, 'ep', split_axis=0, concat_axis=0, tiled=True)  15.5 us
    reduce_scatter x1, waiting for transfers between devices, shards(): lax.psum_scatter(jnp.dot(dense_hidden, dense_down, preferred_element_type...  7.45 us
    all_to_all x1, waiting for transfers between devices, shards(): lax.all_to_all(back_send, 'ep', split_axis=0, concat_axis=0, tiled=True)  7.06 us
    all_gather x1, blocking collectives, shards(): lax.all_gather(tokens, 'tp', axis=1, tiled=True).astype(jnp.float32)  6.46 us
    psum x1, blocking collectives, shards(): squares_out = lax.psum(jnp.sum(combined * combined, axis=1), 'tp')  5.76 us
    dot_general x1, matrix products, shards(): jnp.einsum('erf,efd->erd', hidden, expert_down, preferred_element_type=jn...  5.55 us
    all_to_all x1, starting transfers between devices, shards(): lax.all_to_all(back_send, 'ep', split_axis=0, concat_axis=0, tiled=True)  5.5 us
  transfers between devices with their start and end apart: 3, of which 3 were waited for; matrix products, arithmetic and copies ran while one was open for 8% of the time, Pallas kernels for 0%

commit v1 on v0

v1 whole, which is shorter than its diff:
```python
import functools

import jax
import jax.numpy as jnp
from jax import lax
from jax.experimental import pallas as pl
from jax.experimental.pallas import tpu as pltpu
from jax.sharding import PartitionSpec as P

CAP = 2
CORES = 2
norm_eps = 1e-06
MESH = pl.DeviceIdType.MESH
F32 = jnp.float32
BF16 = jnp.bfloat16


def silu(v):
    return v / (1.0 + jnp.exp(-v))


def kernel(
    n_ep,
    n_tp,
    tok_hbm,
    gain_hbm,
    route_hbm,
    logit_hbm,
    eg_hbm,
    eu_hbm,
    ed_hbm,
    dg_hbm,
    du_hbm,
    dd_hbm,
    mix_hbm,
    og_hbm,
    out_ref,
    tok,
    gain,
    route,
    logit,
    eg,
    eu,
    ed,
    dg,
    du,
    dd,
    mixw,
    og,
    normed,
    placed,
    disp_send,
    disp_recv,
    rows_f,
    dense_send,
    dense_recv,
    pair_send,
    pair_recv,
    summed,
    ret_send,
    ret_recv,
    back,
    sq_send,
    sq_recv,
    lsem,
    ag_s,
    ag_r,
    di_s,
    di_r,
    fw_s,
    fw_r,
    de_s,
    de_r,
    pa_s,
    pa_r,
    re_s,
    re_r,
    sq_s,
    sq_r,
):
    me = lax.axis_index("ep")
    tp = lax.axis_index("tp")
    core = lax.rem(tp, CORES)
    row = lax.div(tp, CORES)
    n_row = n_tp // CORES
    partner = row * CORES + (1 - core)
    n_loc = eg.shape[0]
    t_rows, part = tok.shape[1], tok.shape[2]
    width = part * n_tp
    half = width // CORES
    blk = n_loc * CAP
    slots = n_ep * blk

    def turn(base, d, n):
        return lax.rem(base + d, n)

    def remote(src, dst, s, r, e, t):
        return pltpu.make_async_remote_copy(
            src_ref=src,
            dst_ref=dst,
            send_sem=s,
            recv_sem=r,
            device_id={"ep": e, "tp": t},
            device_id_type=MESH,
        )

    loads = []
    pairs = [
        (tok_hbm, tok.at[tp]),
        (gain_hbm, gain),
        (route_hbm, route),
        (logit_hbm, logit),
        (mix_hbm, mixw),
        (og_hbm, og),
        (dg_hbm, dg),
        (du_hbm, du),
        (dd_hbm, dd),
        (eg_hbm, eg),
        (eu_hbm, eu),
        (ed_hbm, ed),
    ]
    for i, (src, dst) in enumerate(pairs):
        c = pltpu.make_async_copy(src, dst, lsem.at[i])
        c.start()
        loads.append(c)

    barrier = pltpu.get_barrier_semaphore()
    greeted = 0
    for d in range(1, n_ep):
        for y in range(n_row):
            pl.semaphore_signal(
                barrier,
                inc=1,
                device_id={"ep": turn(me, d, n_ep), "tp": y * CORES + core},
                device_id_type=MESH,
            )
            greeted += 1
    for d in range(1, n_tp):
        pl.semaphore_signal(
            barrier, inc=1, device_id={"ep": me, "tp": turn(tp, d, n_tp)}, device_id_type=MESH
        )
        greeted += 1
    pl.semaphore_wait(barrier, greeted)

    loads[0].wait()
    gathers = []
    for d in range(1, n_tp):
        c = remote(tok.at[tp], tok.at[tp], ag_s.at[d], ag_r.at[d], me, turn(tp, d, n_tp))
        c.start()
        gathers.append(c)

    for i in range(1, 6):
        loads[i].wait()
    r0 = route[:, 0:1]
    r1 = route[:, 1:2]
    l0 = logit[:, 0:1]
    l1 = logit[:, 1:2]
    top = jnp.maximum(l0, l1)
    e0 = jnp.exp(l0 - top)
    e1 = jnp.exp(l1 - top)
    w0 = e0 / (e0 + e1)
    w1 = e1 / (e0 + e1)
    slot_e = lax.broadcasted_iota(jnp.int32, (t_rows, slots), 1) // CAP
    slot_c = lax.broadcasted_iota(jnp.int32, (t_rows, slots), 1) % CAP
    hit0 = (slot_e == r0).astype(F32)
    hit1 = (slot_e == r1).astype(F32)
    hits = hit0 + hit1
    ri = lax.broadcasted_iota(jnp.int32, (t_rows, t_rows), 0)
    ci = lax.broadcasted_iota(jnp.int32, (t_rows, t_rows), 1)
    before = jnp.dot((ci < ri).astype(F32), hits, preferred_element_type=F32)
    place = hits * (before == slot_c.astype(F32)).astype(F32)
    combine = place * (hit0 * w0 + hit1 * w1)
    place_t = place.T.astype(BF16)

    for c in gathers:
        c.wait_recv()
    squares = jnp.zeros((t_rows, 1), F32)
    for t in range(n_tp):
        x = tok[t].astype(F32)
        squares += jnp.sum(x * x, axis=1, keepdims=True)
    inv = lax.rsqrt(squares / width + norm_eps)
    mix = jnp.zeros((t_rows, 1), F32)
    for t in range(n_tp):
        cols = pl.ds(t * part, part)
        nx = (tok[t].astype(F32) * inv * gain[:, cols]).astype(BF16)
        normed[:, cols] = nx
        mix += jnp.sum(nx.astype(F32) * mixw[:, cols], axis=1, keepdims=True)
    mix_gate = 1.0 / (1.0 + jnp.exp(-mix))

    my_half = pl.ds(pl.multiple_of(core * half, 128), half)
    placed[...] = jnp.dot(place_t, normed[:, my_half], preferred_element_type=F32)
    for p in range(n_ep):
        disp_send[p] = placed[p * blk : (p + 1) * blk, :].astype(BF16)
    disp_recv[core, me] = disp_send[me]
    sends = []
    for d in range(1, n_ep):
        p = turn(me, d, n_ep)
        c = remote(disp_send.at[p], disp_recv.at[core, me], di_s.at[d], di_r.at[d], p, tp)
        c.start()
        sends.append(c)

    for i in (6, 7, 8):
        loads[i].wait()
    nrm = normed[...]
    dh = (
        silu(jnp.dot(nrm, dg[...], preferred_element_type=F32))
        * jnp.dot(nrm, du[...], preferred_element_type=F32)
    ).astype(BF16)
    dense = []
    for t in range(n_tp):
        dense_send[t] = jnp.dot(
            dh, dd[:, t * part : (t + 1) * part], preferred_element_type=F32
        )
    for d in range(1, n_tp):
        t = turn(tp, d, n_tp)
        c = remote(dense_send.at[t], dense_recv.at[tp], de_s.at[d], de_r.at[d], me, t)
        c.start()
        dense.append(c)
    dense_recv[tp] = dense_send[tp]

    forwards = []
    for d in range(n_ep):
        q = turn(me, n_ep - d, n_ep)
        if d > 0:
            sends[d - 1].wait_recv()
        c = remote(disp_recv.at[core, q], disp_recv.at[core, q], fw_s.at[d], fw_r.at[d], me, partner)
        c.start()
        forwards.append(c)
    for i in (9, 10, 11):
        loads[i].wait()
    for c in forwards:
        c.wait_recv()
    for h in range(CORES):
        for p in range(n_ep):
            rows_f[p * blk : (p + 1) * blk, h * half : (h + 1) * half] = disp_recv[h, p].astype(F32)
    x = rows_f[...].astype(BF16)
    which = (lax.broadcasted_iota(jnp.int32, (slots, 1), 0) % blk) // CAP
    hidden = []
    for e in range(n_loc):
        h = silu(jnp.dot(x, eg[e], preferred_element_type=F32)) * jnp.dot(
            x, eu[e], preferred_element_type=F32
        )
        hidden.append(jnp.where(which == e, h, 0.0).astype(BF16))

    def down(t):
        cols = pl.ds(pl.multiple_of(t * part, 128), part)
        total = jnp.dot(hidden[0], ed[0, :, cols], preferred_element_type=F32)
        for e in range(1, n_loc):
            total += jnp.dot(hidden[e], ed[e, :, cols], preferred_element_type=F32)
        return total

    duo = []
    for y in range(n_row):
        pair_send[y] = down(y * CORES + (1 - core))
        c = remote(pair_send.at[y], pair_recv.at[y], pa_s.at[y], pa_r.at[y], me, partner)
        c.start()
        duo.append(c)
    for y in range(n_row):
        summed[y] = down(y * CORES + core)
    returns = []
    for y in range(n_row):
        duo[y].wait_recv()
        summed[y] += pair_recv[y]
        for p in range(n_ep):
            ret_send[y, p] = summed[y, p * blk : (p + 1) * blk, :]
    for d in range(1, n_ep):
        p = turn(me, d, n_ep)
        for k in range(n_row):
            y = turn(row, k, n_row)
            i = d * n_row + k
            c = remote(
                ret_send.at[y, p],
                ret_recv.at[row, me],
                re_s.at[i],
                re_r.at[i],
                p,
                y * CORES + core,
            )
            c.start()
            returns.append(c)
    for k in range(1, n_row):
        y = turn(row, k, n_row)
        c = remote(
            ret_send.at[y, me], ret_recv.at[row, me], re_s.at[k], re_r.at[k], me, y * CORES + core
        )
        c.start()
        returns.append(c)
    ret_recv[row, me] = ret_send[row, me]

    for c in dense:
        c.wait_recv()
    total = dense_recv[0]
    for t in range(1, n_tp):
        total += dense_recv[t]
    total = mix_gate * total
    for c in returns:
        c.wait_recv()
    for p in range(n_ep):
        s = ret_recv[0, p]
        for y in range(1, n_row):
            s += ret_recv[y, p]
        back[p * blk : (p + 1) * blk, :] = s
    total += jnp.dot(
        combine, back[...], preferred_element_type=F32, precision=lax.Precision.HIGHEST
    )
    sq_send[...] = jnp.broadcast_to(
        jnp.sum(total * total, axis=1, keepdims=True), sq_send.shape
    )
    swaps = []
    for d in range(1, n_tp):
        c = remote(sq_send, sq_recv.at[tp], sq_s.at[d], sq_r.at[d], me, turn(tp, d, n_tp))
        c.start()
        swaps.append(c)
    sq_recv[tp] = sq_send[...]
    for c in swaps:
        c.wait_recv()
    all_sq = sq_recv[0]
    for t in range(1, n_tp):
        all_sq += sq_recv[t]
    scale = lax.rsqrt(all_sq[:, 0:1] / width + norm_eps)
    out_ref[...] = (total * scale * og[...]).astype(out_ref.dtype)
    for c in gathers + sends + dense + forwards + duo + returns + swaps:
        c.wait_send()


def shards(n_ep, n_tp, *args):
    (tok, gain, route, logit, eg, eu, ed, dg, du, dd, mixw, og) = args
    t_rows, part = tok.shape
    width = part * n_tp
    n_loc, _, ff = eg.shape
    n_row = n_tp // CORES
    half = width // CORES
    blk = n_loc * CAP
    slots = n_ep * blk
    dma = pltpu.SemaphoreType.DMA
    V = pltpu.VMEM
    scratch = [
        V((n_tp, t_rows, part), BF16),
        V((1, width), F32),
        V(route.shape, jnp.int32),
        V(logit.shape, F32),
        V(eg.shape, BF16),
        V(eu.shape, BF16),
        V(ed.shape, BF16),
        V(dg.shape, BF16),
        V(du.shape, BF16),
        V(dd.shape, BF16),
        V((1, width), F32),
        V((1, part), F32),
        V((t_rows, width), BF16),
        V((slots, half), F32),
        V((n_ep, blk, half), BF16),
        V((CORES, n_ep, blk, half), BF16),
        V((slots, width), F32),
        V((n_tp, t_rows, part), F32),
        V((n_tp, t_rows, part), F32),
        V((n_row, slots, part), F32),
        V((n_row, slots, part), F32),
        V((n_row, slots, part), F32),
        V((n_row, n_ep, blk, part), F32),
        V((n_row, n_ep, blk, part), F32),
        V((slots, part), F32),
        V((t_rows, 128), F32),
        V((n_tp, t_rows, 128), F32),
        dma((12,)),
        dma((n_tp,)),
        dma((n_tp,)),
        dma((n_ep,)),
        dma((n_ep,)),
        dma((n_ep,)),
        dma((n_ep,)),
        dma((n_tp,)),
        dma((n_tp,)),
        dma((n_row,)),
        dma((n_row,)),
        dma((n_ep * n_row,)),
        dma((n_ep * n_row,)),
        dma((n_tp,)),
        dma((n_tp,)),
    ]
    return pl.pallas_call(
        functools.partial(kernel, n_ep, n_tp),
        out_shape=jax.ShapeDtypeStruct((t_rows, part), BF16),
        in_specs=[pl.BlockSpec(memory_space=pltpu.HBM)] * 12,
        out_specs=pl.BlockSpec(memory_space=pltpu.VMEM),
        scratch_shapes=scratch,
        compiler_params=pltpu.CompilerParams(
            collective_id=0, has_side_effects=True, vmem_limit_bytes=60 * 1024 * 1024
        ),
        name="moe_layer",
    )(
        tok,
        gain.reshape(1, width),
        route,
        logit,
        eg,
        eu,
        ed,
        dg,
        du,
        dd,
        mixw.reshape(1, width),
        og.reshape(1, part),
    )


def solution(mesh):
    placed = (
        P("ep", "tp"),
        P(),
        P("ep", None),
        P("ep", None),
        P("ep", None, "tp"),
        P("ep", None, "tp"),
        P("ep", "tp", None),
        P(None, "tp"),
        P(None, "tp"),
        P("tp", None),
        P(),
        P("tp"),
    )
    return jax.shard_map(
        functools.partial(shards, mesh.shape["ep"], mesh.shape["tp"]),
        mesh=mesh,
        in_specs=placed,
        out_specs=P("ep", "tp"),
        check_vma=False,
    )
```

time: 101 us -> 34.2 us (0.34)
  waiting for transfers between devices: 30.4 us -> 0 us
  Pallas kernels: 0 us -> 29.9 us
  blocking collectives: 27.7 us -> 0 us
  matrix products: 16.3 us -> 0 us
  between operations: 13.5 us -> 0.01 us
  starting transfers between devices: 5.54 us -> 0 us
  other arithmetic: 3.46 us -> 0 us
    pallas_call x0 -> x1, Pallas kernels: none -> 29.9 us  [shards(): pl.pallas_call(functools.partial(kernel, n_ep, n_tp), out_shape=jax.Shape...]
    reduce_scatter x2 -> x0, waiting for transfers between devices: 23.3 us -> none  [the longest x1 15.9 us: shards(): lax.psum_scatter(partial_value, 'tp', scatter_dimension=2, tiled=True)]
    dot_general x7 -> x0, matrix products: 16.3 us -> none  [the longest x1 5.55 us: shards(): jnp.einsum('erf,efd->erd', hidden, expert_down, preferred_element_type=jn...]
    all_to_all x1 -> x0, blocking collectives: 15.5 us -> none  [shards(): lax.all_to_all(outgoing, 'ep', split_axis=0, concat_axis=0, tiled=True)]
    all_to_all x1 -> x0, waiting for transfers between devices: 7.06 us -> none  [shards(): lax.all_to_all(back_send, 'ep', split_axis=0, concat_axis=0, tiled=True)]
    all_gather x1 -> x0, blocking collectives: 6.46 us -> none  [shards(): lax.all_gather(tokens, 'tp', axis=1, tiled=True).astype(jnp.float32)]
    psum x1 -> x0, blocking collectives: 5.76 us -> none  [shards(): squares_out = lax.psum(jnp.sum(combined * combined, axis=1), 'tp')]
    all_to_all x1 -> x0, starting transfers between devices: 5.5 us -> none  [shards(): lax.all_to_all(back_send, 'ep', split_axis=0, concat_axis=0, tiled=True)]
  transfers between devices with their start and end apart: 3 -> 0, of which waited for: 3 -> 0; matrix products, arithmetic and copies ran while one was open for 8% -> 0% of each run, Pallas kernels for 0% -> 0%
where the time goes in v1:
time: 34.2 us; the launch traced here: 33.9 us
  Pallas kernels  29.9 us (87%)
  local copies, waits for them, and re-layouts  4.01 us (12%)
    pallas_call x1, Pallas kernels, shards(): pl.pallas_call(functools.partial(kernel, n_ep, n_tp), out_shape=jax.Shape...  29.9 us
    unnamed x3, local copies, waits for them, and re-layouts  4.01 us

profile of v1, /device:TPU:0, one launch (start us, length us, event | category | flops | bytes accessed | tf_op | source)
XLA Modules:
  0.0 33.9 jit_solution(6650715800609330436)
XLA Ops:
  0.0 1.3 %copy.13.route_hbm = s32[8,2]{1,0:T(8,128)} copy(s32[8,2]{0,1:T(2,128)} %param.14) | data formatting | bytes 128 | tf_op args[2]
  1.3 1.3 %copy.14.logit_hbm = f32[8,2]{1,0:T(8,128)} copy(f32[8,2]{0,1:T(2,128)} %param.15) | data formatting | bytes 128 | tf_op args[3]
  2.7 29.9 %moe_layer.1 = bf16[8,1024]{1,0:T(8,128)(2,1)} custom-call(bf16[8,1024]{1,0:T(8,128)(2,1)} %tok_hbm.1, f32[1,4096]{1,0:T(1,128)} %bitcast.3, s32[8,2]{1,0:T(8,128)} %copy.13.route_hbm, f32[8,2]{1,0:T(8,128)} %copy.14.logit_hbm, bf16[2,4096,256]{2,1,0:T(8,128)(2,1)} %eg_hbm.1, bf16[2,4096,256]{2,1,0:T(8,128)(2,1)} %eu_hbm.1, bf16[2,256,4096]{2,1,0:T(8,128)(2,1)} %ed_hbm.1, ...), custom_call_target="tpu_custom_call" | custom-call | tf_op jit(solution)/shard_map/moe_layer/pallas_call | solution.py:381
  32.6 1.3 %copy.16 = bf16[8,1024]{1,0:T(8,128)(2,1)} copy(bf16[8,1024]{1,0:T(8,128)(2,1)} %moe_layer.1) | data formatting | bytes 32768

commit v2 on v1

--- a/solution.py
+++ b/solution.py
@@ -52,6 +52,7 @@
     disp_send,
     disp_recv,
     rows_f,
+    rows_n,
     dense_send,
     dense_recv,
     pair_send,
@@ -87,7 +88,6 @@
     n_loc = eg.shape[0]
     t_rows, part = tok.shape[1], tok.shape[2]
     width = part * n_tp
-    half = width // CORES
     blk = n_loc * CAP
     slots = n_ep * blk
 
@@ -142,35 +142,66 @@
         greeted += 1
     pl.semaphore_wait(barrier, greeted)
 
+    near = sorted(range(1, n_ep), key=lambda d: min(d, n_ep - d))
+
     loads[0].wait()
     gathers = []
     for d in range(1, n_tp):
-        c = remote(tok.at[tp], tok.at[tp], ag_s.at[d], ag_r.at[d], me, turn(tp, d, n_tp))
-        c.start()
-        gathers.append(c)
-
-    for i in range(1, 6):
+        gathers.append(
+            remote(tok.at[tp], tok.at[tp], ag_s.at[d], ag_r.at[d], me, turn(tp, d, n_tp))
+        )
+
+    loads[2].wait()
+    r0 = route[0:1, :]
+    r1 = route[1:2, :]
+    slot = lax.broadcasted_iota(jnp.int32, (slots, t_rows), 0)
+    slot_e = slot // CAP
+    slot_c = slot % CAP
+    hit0 = (slot_e == r0).astype(F32)
+    hit1 = (slot_e == r1).astype(F32)
+    hits = hit0 + hit1
+    ri = lax.broadcasted_iota(jnp.int32, (t_rows, t_rows), 0)
+    ci = lax.broadcasted_iota(jnp.int32, (t_rows, t_rows), 1)
+    before = jnp.dot(hits, (ri < ci).astype(F32), preferred_element_type=F32)
+    place_t = hits * (before == slot_c.astype(F32)).astype(F32)
+
+    placed[...] = jnp.dot(place_t.astype(BF16), tok[tp], preferred_element_type=F32)
+    for p in range(n_ep):
+        disp_send[p] = placed[p * blk : (p + 1) * blk, :].astype(BF16)
+    sends = {}
+    for d in reversed(near):
+        p = turn(me, d, n_ep)
+        c = remote(disp_send.at[p], disp_recv.at[tp, me], di_s.at[d], di_r.at[d], p, tp)
+        c.start()
+        sends[d] = c
+    disp_recv[tp, me] = disp_send[me]
+    for c in gathers:
+        c.start()
+
+    for d in [0] + near:
+        q = turn(me, n_ep - d, n_ep)
+        if d > 0:
+            sends[d].wait_recv()
+        for k in range(1, n_tp):
+            remote(
+                disp_recv.at[tp, q],
+                disp_recv.at[tp, q],
+                fw_s.at[k],
+                fw_r.at[k],
+                me,
+                turn(tp, k, n_tp),
+            ).start()
+
+    for i in (1, 3, 4, 5):
         loads[i].wait()
-    r0 = route[:, 0:1]
-    r1 = route[:, 1:2]
-    l0 = logit[:, 0:1]
-    l1 = logit[:, 1:2]
+    l0 = logit[0:1, :]
+    l1 = logit[1:2, :]
     top = jnp.maximum(l0, l1)
     e0 = jnp.exp(l0 - top)
     e1 = jnp.exp(l1 - top)
     w0 = e0 / (e0 + e1)
     w1 = e1 / (e0 + e1)
-    slot_e = lax.broadcasted_iota(jnp.int32, (t_rows, slots), 1) // CAP
-    slot_c = lax.broadcasted_iota(jnp.int32, (t_rows, slots), 1) % CAP
-    hit0 = (slot_e == r0).astype(F32)
-    hit1 = (slot_e == r1).astype(F32)
-    hits = hit0 + hit1
-    ri = lax.broadcasted_iota(jnp.int32, (t_rows, t_rows), 0)
-    ci = lax.broadcasted_iota(jnp.int32, (t_rows, t_rows), 1)
-    before = jnp.dot((ci < ri).astype(F32), hits, preferred_element_type=F32)
-    place = hits * (before == slot_c.astype(F32)).astype(F32)
-    combine = place * (hit0 * w0 + hit1 * w1)
-    place_t = place.T.astype(BF16)
+    combine = (place_t * (hit0 * w0 + hit1 * w1)).T
 
     for c in gathers:
         c.wait_recv()
@@ -187,18 +218,6 @@
         mix += jnp.sum(nx.astype(F32) * mixw[:, cols], axis=1, keepdims=True)
     mix_gate = 1.0 / (1.0 + jnp.exp(-mix))
 
-    my_half = pl.ds(pl.multiple_of(core * half, 128), half)
-    placed[...] = jnp.dot(place_t, normed[:, my_half], preferred_element_type=F32)
-    for p in range(n_ep):
-        disp_send[p] = placed[p * blk : (p + 1) * blk, :].astype(BF16)
-    disp_recv[core, me] = disp_send[me]
-    sends = []
-    for d in range(1, n_ep):
-        p = turn(me, d, n_ep)
-        c = remote(disp_send.at[p], disp_recv.at[core, me], di_s.at[d], di_r.at[d], p, tp)
-        c.start()
-        sends.append(c)
-
     for i in (6, 7, 8):
         loads[i].wait()
     nrm = normed[...]
@@ -218,22 +237,32 @@
         dense.append(c)
     dense_recv[tp] = dense_send[tp]
 
-    forwards = []
-    for d in range(n_ep):
-        q = turn(me, n_ep - d, n_ep)
-        if d > 0:
-            sends[d - 1].wait_recv()
-        c = remote(disp_recv.at[core, q], disp_recv.at[core, q], fw_s.at[d], fw_r.at[d], me, partner)
-        c.start()
-        forwards.append(c)
     for i in (9, 10, 11):
         loads[i].wait()
-    for c in forwards:
+    forwards = []
+    for k in range(1, n_tp):
+        c = remote(
+            disp_recv.at[tp],
+            disp_recv.at[turn(tp, n_tp - k, n_tp)],
+            fw_s.at[k],
+            fw_r.at[k],
+            me,
+            turn(tp, k, n_tp),
+        )
         c.wait_recv()
-    for h in range(CORES):
+        forwards.append(c)
+    squares = jnp.zeros((slots, 1), F32)
+    for t in range(n_tp):
+        cols = pl.ds(t * part, part)
         for p in range(n_ep):
-            rows_f[p * blk : (p + 1) * blk, h * half : (h + 1) * half] = disp_recv[h, p].astype(F32)
-    x = rows_f[...].astype(BF16)
+            rows_f[p * blk : (p + 1) * blk, cols] = disp_recv[t, p].astype(F32)
+        x = rows_f[:, cols]
+        squares += jnp.sum(x * x, axis=1, keepdims=True)
+    inv = lax.rsqrt(squares / width + norm_eps)
+    for t in range(n_tp):
+        cols = pl.ds(t * part, part)
+        rows_n[:, cols] = (rows_f[:, cols] * inv * gain[:, cols]).astype(BF16)
+    x = rows_n[...]
     which = (lax.broadcasted_iota(jnp.int32, (slots, 1), 0) % blk) // CAP
     hidden = []
     for e in range(n_loc):
@@ -319,7 +348,7 @@
         all_sq += sq_recv[t]
     scale = lax.rsqrt(all_sq[:, 0:1] / width + norm_eps)
     out_ref[...] = (total * scale * og[...]).astype(out_ref.dtype)
-    for c in gathers + sends + dense + forwards + duo + returns + swaps:
+    for c in gathers + list(sends.values()) + dense + forwards + duo + returns + swaps:
         c.wait_send()
 
 
@@ -329,7 +358,6 @@
     width = part * n_tp
     n_loc, _, ff = eg.shape
     n_row = n_tp // CORES
-    half = width // CORES
     blk = n_loc * CAP
     slots = n_ep * blk
     dma = pltpu.SemaphoreType.DMA
@@ -337,8 +365,8 @@
     scratch = [
         V((n_tp, t_rows, part), BF16),
         V((1, width), F32),
-        V(route.shape, jnp.int32),
-        V(logit.shape, F32),
+        V(route.shape[::-1], jnp.int32),
+        V(logit.shape[::-1], F32),
         V(eg.shape, BF16),
         V(eu.shape, BF16),
         V(ed.shape, BF16),
@@ -348,10 +376,11 @@
         V((1, width), F32),
         V((1, part), F32),
         V((t_rows, width), BF16),
-        V((slots, half), F32),
-        V((n_ep, blk, half), BF16),
-        V((CORES, n_ep, blk, half), BF16),
+        V((slots, part), F32),
+        V((n_ep, blk, part), BF16),
+        V((n_tp, n_ep, blk, part), BF16),
         V((slots, width), F32),
+        V((slots, width), BF16),
         V((n_tp, t_rows, part), F32),
         V((n_tp, t_rows, part), F32),
         V((n_row, slots, part), F32),
@@ -367,8 +396,8 @@
         dma((n_tp,)),
         dma((n_ep,)),
         dma((n_ep,)),
-        dma((n_ep,)),
-        dma((n_ep,)),
+        dma((n_tp,)),
+        dma((n_tp,)),
         dma((n_tp,)),
         dma((n_tp,)),
         dma((n_row,)),
@@ -391,8 +420,8 @@
     )(
         tok,
         gain.reshape(1, width),
-        route,
-        logit,
+        route.T,
+        logit.T,
         eg,
         eu,
         ed,

time: 34.2 us -> 30.1 us (0.88)
  local copies, waits for them, and re-layouts: 4.01 us -> 1.32 us
  Pallas kernels: 29.9 us -> 28.5 us
    unnamed x3 -> x1, local copies, waits for them, and re-layouts: 4.01 us -> 1.32 us
    pallas_call x1, Pallas kernels: 29.9 us -> 28.5 us  [shards(): pl.pallas_call(functools.partial(kernel, n_ep, n_tp), out_shape=jax.Shape...]
where the time goes in v2:
time: 30.1 us; the launch traced here: 29.9 us
  Pallas kernels  28.5 us (95%)
  local copies, waits for them, and re-layouts  1.32 us (4%)
    pallas_call x1, Pallas kernels, shards(): pl.pallas_call(functools.partial(kernel, n_ep, n_tp), out_shape=jax.Shape...  28.5 us
    unnamed x1, local copies, waits for them, and re-layouts  1.32 us

profile of v2, /device:TPU:0, one launch (start us, length us, event | category | flops | bytes accessed | tf_op | source)
XLA Modules:
  0.0 29.9 jit_solution(13476768843331225285)
XLA Ops:
  0.0 28.5 %moe_layer.1 = bf16[8,1024]{1,0:T(8,128)(2,1)} custom-call(bf16[8,1024]{1,0:T(8,128)(2,1)} %tok_hbm.1, f32[1,4096]{1,0:T(1,128)} %bitcast.5, s32[2,8]{1,0:T(2,128)} %bitcast.8, f32[2,8]{1,0:T(2,128)} %bitcast.9, bf16[2,4096,256]{2,1,0:T(8,128)(2,1)} %eg_hbm.1, bf16[2,4096,256]{2,1,0:T(8,128)(2,1)} %eu_hbm.1, bf16[2,256,4096]{2,1,0:T(8,128)(2,1)} %ed_hbm.1, ...), custom_call_target="tpu_custom_call" | custom-call | tf_op jit(solution)/shard_map/moe_layer/pallas_call | solution.py:410
  28.6 1.3 %copy.14 = bf16[8,1024]{1,0:T(8,128)(2,1)} copy(bf16[8,1024]{1,0:T(8,128)(2,1)} %moe_layer.1) | data formatting | bytes 32768

commit v3 on v2

--- a/solution.py
+++ b/solution.py
@@ -10,6 +10,7 @@
 CAP = 2
 CORES = 2
 norm_eps = 1e-06
+LOG2E = 1.4426950408889634
 MESH = pl.DeviceIdType.MESH
 F32 = jnp.float32
 BF16 = jnp.bfloat16
@@ -58,6 +59,7 @@
     pair_send,
     pair_recv,
     summed,
+    coded,
     ret_send,
     ret_recv,
     back,
@@ -289,9 +291,17 @@
     returns = []
     for y in range(n_row):
         duo[y].wait_recv()
-        summed[y] += pair_recv[y]
+        v = summed[y] + pair_recv[y]
+        peak = jnp.max(jnp.abs(v), axis=1, keepdims=True)
+        power = jnp.ceil(jnp.log(jnp.maximum(peak, 1e-30)) * LOG2E)
+        coded[:, 0:part] = jnp.clip(
+            jnp.floor(v * jnp.exp2(15.0 - power) + 0.5), -32767.0, 32767.0
+        )
+        coded[:, part : part + 128] = jnp.broadcast_to(power, (slots, 128))
         for p in range(n_ep):
-            ret_send[y, p] = summed[y, p * blk : (p + 1) * blk, :]
+            ret_send[y, p] = (
+                coded[p * blk : (p + 1) * blk, :].astype(jnp.int32).astype(jnp.int16)
+            )
     for d in range(1, n_ep):
         p = turn(me, d, n_ep)
         for k in range(n_row):
@@ -324,13 +334,15 @@
     total = mix_gate * total
     for c in returns:
         c.wait_recv()
-    for p in range(n_ep):
-        s = ret_recv[0, p]
-        for y in range(1, n_row):
-            s += ret_recv[y, p]
-        back[p * blk : (p + 1) * blk, :] = s
+    mixed = jnp.zeros((slots, part), F32)
+    for y in range(n_row):
+        for p in range(n_ep):
+            back[y, p * blk : (p + 1) * blk, :] = (
+                ret_recv[y, p].astype(jnp.int32).astype(F32)
+            )
+        mixed += back[y, :, 0:part] * jnp.exp2(back[y, :, part : part + 1] - 15.0)
     total += jnp.dot(
-        combine, back[...], preferred_element_type=F32, precision=lax.Precision.HIGHEST
+        combine, mixed, preferred_element_type=F32, precision=lax.Precision.HIGHEST
     )
     sq_send[...] = jnp.broadcast_to(
         jnp.sum(total * total, axis=1, keepdims=True), sq_send.shape
@@ -386,9 +398,10 @@
         V((n_row, slots, part), F32),
         V((n_row, slots, part), F32),
         V((n_row, slots, part), F32),
-        V((n_row, n_ep, blk, part), F32),
-        V((n_row, n_ep, blk, part), F32),
-        V((slots, part), F32),
+        V((slots, part + 128), F32),
+        V((n_row, n_ep, blk, part + 128), jnp.int16),
+        V((n_row, n_ep, blk, part + 128), jnp.int16),
+        V((n_row, slots, part + 128), F32),
         V((t_rows, 128), F32),
         V((n_tp, t_rows, 128), F32),
         dma((12,)),

time: 30.1 us -> 29.1 us (0.967)
  Pallas kernels: 28.5 us -> 27.5 us
    pallas_call x1, Pallas kernels: 28.5 us -> 27.5 us  [shards(): pl.pallas_call(functools.partial(kernel, n_ep, n_tp), out_shape=jax.Shape...]
where the time goes in v3:
time: 29.1 us; the launch traced here: 28.9 us
  Pallas kernels  27.5 us (95%)
  local copies, waits for them, and re-layouts  1.32 us (5%)
    pallas_call x1, Pallas kernels, shards(): pl.pallas_call(functools.partial(kernel, n_ep, n_tp), out_shape=jax.Shape...  27.5 us
    unnamed x1, local copies, waits for them, and re-layouts  1.32 us

profile of v3, /device:TPU:0, one launch (start us, length us, event | category | flops | bytes accessed | tf_op | source)
XLA Modules:
  0.0 28.9 jit_solution(10184103907204240107)
XLA Ops:
  0.0 27.5 %moe_layer.1 = bf16[8,1024]{1,0:T(8,128)(2,1)} custom-call(bf16[8,1024]{1,0:T(8,128)(2,1)} %tok_hbm.1, f32[1,4096]{1,0:T(1,128)} %bitcast.5, s32[2,8]{1,0:T(2,128)} %bitcast.8, f32[2,8]{1,0:T(2,128)} %bitcast.9, bf16[2,4096,256]{2,1,0:T(8,128)(2,1)} %eg_hbm.1, bf16[2,4096,256]{2,1,0:T(8,128)(2,1)} %eu_hbm.1, bf16[2,256,4096]{2,1,0:T(8,128)(2,1)} %ed_hbm.1, ...), custom_call_target="tpu_custom_call" | custom-call | tf_op jit(solution)/shard_map/moe_layer/pallas_call | solution.py:423
  27.6 1.3 %copy.14 = bf16[8,1024]{1,0:T(8,128)(2,1)} copy(bf16[8,1024]{1,0:T(8,128)(2,1)} %moe_layer.1) | data formatting | bytes 32768

commit v4 on v3

--- a/solution.py
+++ b/solution.py
@@ -106,6 +106,19 @@
             device_id_type=MESH,
         )
 
+    barrier = pltpu.get_barrier_semaphore()
+    greeted = 0
+    for d in range(1, n_ep):
+        pl.semaphore_signal(
+            barrier, inc=1, device_id={"ep": turn(me, d, n_ep), "tp": tp}, device_id_type=MESH
+        )
+        greeted += 1
+    for d in range(1, n_tp):
+        pl.semaphore_signal(
+            barrier, inc=1, device_id={"ep": me, "tp": turn(tp, d, n_tp)}, device_id_type=MESH
+        )
+        greeted += 1
+
     loads = []
     pairs = [
         (tok_hbm, tok.at[tp]),
@@ -126,24 +139,6 @@
         c.start()
         loads.append(c)
 
-    barrier = pltpu.get_barrier_semaphore()
-    greeted = 0
-    for d in range(1, n_ep):
-        for y in range(n_row):
-            pl.semaphore_signal(
-                barrier,
-                inc=1,
-                device_id={"ep": turn(me, d, n_ep), "tp": y * CORES + core},
-                device_id_type=MESH,
-            )
-            greeted += 1
-    for d in range(1, n_tp):
-        pl.semaphore_signal(
-            barrier, inc=1, device_id={"ep": me, "tp": turn(tp, d, n_tp)}, device_id_type=MESH
-        )
-        greeted += 1
-    pl.semaphore_wait(barrier, greeted)
-
     near = sorted(range(1, n_ep), key=lambda d: min(d, n_ep - d))
 
     loads[0].wait()
@@ -170,13 +165,26 @@
     placed[...] = jnp.dot(place_t.astype(BF16), tok[tp], preferred_element_type=F32)
     for p in range(n_ep):
         disp_send[p] = placed[p * blk : (p + 1) * blk, :].astype(BF16)
+    for i in (1, 3, 4, 5):
+        loads[i].wait()
+    l0 = logit[0:1, :]
+    l1 = logit[1:2, :]
+    top = jnp.maximum(l0, l1)
+    e0 = jnp.exp(l0 - top)
+    e1 = jnp.exp(l1 - top)
+    w0 = e0 / (e0 + e1)
+    w1 = e1 / (e0 + e1)
+    combine = (place_t * (hit0 * w0 + hit1 * w1)).T
+
+    disp_recv[tp, me] = disp_send[me]
+
+    pl.semaphore_wait(barrier, greeted)
     sends = {}
     for d in reversed(near):
         p = turn(me, d, n_ep)
         c = remote(disp_send.at[p], disp_recv.at[tp, me], di_s.at[d], di_r.at[d], p, tp)
         c.start()
         sends[d] = c
-    disp_recv[tp, me] = disp_send[me]
     for c in gathers:
         c.start()
 
@@ -193,17 +201,6 @@
                 me,
                 turn(tp, k, n_tp),
             ).start()
-
-    for i in (1, 3, 4, 5):
-        loads[i].wait()
-    l0 = logit[0:1, :]
-    l1 = logit[1:2, :]
-    top = jnp.maximum(l0, l1)
-    e0 = jnp.exp(l0 - top)
-    e1 = jnp.exp(l1 - top)
-    w0 = e0 / (e0 + e1)
-    w1 = e1 / (e0 + e1)
-    combine = (place_t * (hit0 * w0 + hit1 * w1)).T
 
     for c in gathers:
         c.wait_recv()
@@ -220,26 +217,14 @@
         mix += jnp.sum(nx.astype(F32) * mixw[:, cols], axis=1, keepdims=True)
     mix_gate = 1.0 / (1.0 + jnp.exp(-mix))
 
-    for i in (6, 7, 8):
+    for i in (6, 7):
         loads[i].wait()
     nrm = normed[...]
     dh = (
         silu(jnp.dot(nrm, dg[...], preferred_element_type=F32))
         * jnp.dot(nrm, du[...], preferred_element_type=F32)
     ).astype(BF16)
-    dense = []
-    for t in range(n_tp):
-        dense_send[t] = jnp.dot(
-            dh, dd[:, t * part : (t + 1) * part], preferred_element_type=F32
-        )
-    for d in range(1, n_tp):
-        t = turn(tp, d, n_tp)
-        c = remote(dense_send.at[t], dense_recv.at[tp], de_s.at[d], de_r.at[d], me, t)
-        c.start()
-        dense.append(c)
-    dense_recv[tp] = dense_send[tp]
-
-    for i in (9, 10, 11):
+    for i in (8, 9, 10, 11):
         loads[i].wait()
     forwards = []
     for k in range(1, n_tp):
@@ -325,6 +310,18 @@
         c.start()
         returns.append(c)
     ret_recv[row, me] = ret_send[row, me]
+
+    dense = []
+    for t in range(n_tp):
+        dense_send[t] = jnp.dot(
+            dh, dd[:, t * part : (t + 1) * part], preferred_element_type=F32
+        )
+    for d in range(1, n_tp):
+        t = turn(tp, d, n_tp)
+        c = remote(dense_send.at[t], dense_recv.at[tp], de_s.at[d], de_r.at[d], me, t)
+        c.start()
+        dense.append(c)
+    dense_recv[tp] = dense_send[tp]
 
     for c in dense:
         c.wait_recv()

time: 29.1 us -> 28.8 us (0.990)
  Pallas kernels: 27.5 us -> 27.2 us
    pallas_call x1, Pallas kernels: 27.5 us -> 27.2 us  [shards(): pl.pallas_call(functools.partial(kernel, n_ep, n_tp), out_shape=jax.Shape...]
where the time goes in v4:
time: 28.8 us; the launch traced here: 28.5 us
  Pallas kernels  27.2 us (94%)
  local copies, waits for them, and re-layouts  1.32 us (5%)
    pallas_call x1, Pallas kernels, shards(): pl.pallas_call(functools.partial(kernel, n_ep, n_tp), out_shape=jax.Shape...  27.2 us
    unnamed x1, local copies, waits for them, and re-layouts  1.32 us

profile of v4, /device:TPU:0, one launch (start us, length us, event | category | flops | bytes accessed | tf_op | source)
XLA Modules:
  0.0 28.5 jit_solution(15689329826456150217)
XLA Ops:
  0.0 27.2 %moe_layer.1 = bf16[8,1024]{1,0:T(8,128)(2,1)} custom-call(bf16[8,1024]{1,0:T(8,128)(2,1)} %tok_hbm.1, f32[1,4096]{1,0:T(1,128)} %bitcast.5, s32[2,8]{1,0:T(2,128)} %bitcast.8, f32[2,8]{1,0:T(2,128)} %bitcast.9, bf16[2,4096,256]{2,1,0:T(8,128)(2,1)} %eg_hbm.1, bf16[2,4096,256]{2,1,0:T(8,128)(2,1)} %eu_hbm.1, bf16[2,256,4096]{2,1,0:T(8,128)(2,1)} %ed_hbm.1, ...), custom_call_target="tpu_custom_call" | custom-call | tf_op jit(solution)/shard_map/moe_layer/pallas_call | solution.py:420
  27.2 1.3 %copy.14 = bf16[8,1024]{1,0:T(8,128)(2,1)} copy(bf16[8,1024]{1,0:T(8,128)(2,1)} %moe_layer.1) | data formatting | bytes 32768
